TPU v7x, 512 devices: a 4x2x32 block of a 4x8x32 slice. The times are simulated.
512 devices in a mesh: grp: 2 (over y), fs: 32 (over z), tp: 8 (over x, core).
Axes of the slice: x: 4, y: 2, z: 32, core: 2. Of those that a mesh axis runs over, the one named last changes fastest.
The devices are a block of a 4x8x32 slice.
Arguments:
- tokens: bfloat16 [24576, 2048], P(('grp', 'fs'), 'tp'), parts along dimension 0, may hold values from -6 to 6
- mix_gain: float32 [2048], replicated, may hold values from 0.1 to 1.9
- w_signal: bfloat16 [2048, 1024], P('fs', 'tp'), may hold values from -0.125 to 0.125
- w_outer_gate: bfloat16 [2048, 1024], P('fs', 'tp'), may hold values from -0.125 to 0.125
- w_inner_gate: bfloat16 [2048, 1024], P('fs', 'tp'), may hold values from -0.125 to 0.125
- mix_taps: float32 [3, 1024], P(None, 'tp'), may hold values from -3 to 3
- w_mix_out: bfloat16 [1024, 2048], P('tp', 'fs'), may hold values from -0.1875 to 0.1875
- ffn_gain: float32 [2048], replicated, may hold values from 0.1 to 1.9
- w_gate: bfloat16 [2048, 5120], P('fs', 'tp'), may hold values from -0.125 to 0.125
- w_value: bfloat16 [2048, 5120], P('fs', 'tp'), may hold values from -0.125 to 0.125
- up_taps: float32 [2, 3, 5120], P(None, None, 'tp'), may hold values from -3 to 3
- up_bias: float32 [2, 5120], P(None, 'tp'), may hold values from -3 to 3
- w_down: bfloat16 [5120, 2048], P('tp', 'fs'), may hold values from -0.078125 to 0.078125
Outputs:
- layer_out: bfloat16 [24576, 2048], P(('grp', 'fs'), 'tp'), parts along dimension 0
There are 2 independent parts, one for each index of `grp`. A program takes and returns all parts, laid end to end along the dimension named above; an argument that names none is the same for every part. Nothing has to cross between parts.
All inputs are finite; a program needn't handle non-finite values.
Results may differ from a plain program's by a relative error of at most 0.022.
Values may be sent and summed in bfloat16 or wider, within the bound.
A program may use at most 64 MiB of HBM per device.

v0:
```python
import jax
import jax.numpy as jnp
from jax import lax
from jax.sharding import PartitionSpec as P

SEQS_DEV = 2


def in_one_piece(arrays, axis, dim, along):
    widths = [a.shape[along] for a in arrays]
    both = jnp.concatenate(arrays, axis=along)
    filled = lax.all_gather(both, axis, axis=dim, tiled=True)
    return tuple(jnp.split(filled, [sum(widths[:k]) for k in range(1, len(widths))], axis=along))


def copy_for_each(value, axis):
    copies = jnp.broadcast_to(value, (lax.axis_size(axis), *value.shape))
    return lax.all_to_all(copies, axis, split_axis=0, concat_axis=0, tiled=True)


def in_order(pieces, dim):
    shape = list(pieces.shape[1:])
    shape[dim] *= pieces.shape[0]
    return jnp.moveaxis(pieces, 0, dim).reshape(shape)


def gathered_copies(value, axis, dim):
    pieces = copy_for_each(value, axis)
    return in_order(pieces, dim)


def split_up(value, dim, devices):
    shape = value.shape
    pieces = value.reshape(*shape[:dim], devices, shape[dim] // devices, *shape[dim + 1 :])
    return jnp.moveaxis(pieces, dim, 0)


def sent_and_summed(value, axis, dim):
    devices = lax.axis_size(axis)
    pieces = lax.all_to_all(split_up(value, dim, devices), axis, 0, 0, tiled=True)
    return jnp.sum(pieces.astype(jnp.float32), axis=0)


def conv_positions(values, taps):
    width = values.shape[1]
    blocks = values.reshape(SEQS_DEV, -1, width)
    length = blocks.shape[1]
    padded = jnp.pad(blocks, ((0, 0), (2, 0), (0, 0)))
    result = (
        padded[:, 0:length] * taps[0]
        + padded[:, 1 : length + 1] * taps[1]
        + padded[:, 2 : length + 2] * taps[2]
    )
    return result.reshape(-1, width)


def rms_norm(stream, gain):
    values = stream.astype(jnp.float32)
    scale = lax.rsqrt(jnp.mean(values * values, axis=-1, keepdims=True) + 1e-06)
    return (values * scale * gain).astype(jnp.bfloat16)


def on_device(
    tokens,
    mix_gain,
    w_signal,
    w_outer_gate,
    w_inner_gate,
    mix_taps,
    w_mix_out,
    ffn_gain,
    w_gate,
    w_value,
    up_taps,
    up_bias,
    w_down,
):
    gate_full, value_full = in_one_piece((w_gate, w_value), "fs", 0, 1)
    whole = gathered_copies(tokens, "tp", 1)
    normed = rms_norm(whole, mix_gain)
    signal_full, outer_full, inner_full = in_one_piece(
        (w_signal, w_outer_gate, w_inner_gate), "fs", 0, 1
    )
    signal = jnp.dot(normed, signal_full, preferred_element_type=jnp.float32)
    outer = jnp.dot(normed, outer_full, preferred_element_type=jnp.float32)
    inner = jnp.dot(normed, inner_full, preferred_element_type=jnp.float32)
    signal = signal.astype(jnp.bfloat16).astype(jnp.float32)
    outer = outer.astype(jnp.bfloat16).astype(jnp.float32)
    inner = inner.astype(jnp.bfloat16).astype(jnp.float32)
    mixed = (outer * conv_positions(inner * signal, mix_taps)).astype(jnp.bfloat16)
    mix_terms = jnp.dot(
        mixed,
        lax.all_gather(w_mix_out, "fs", axis=1, tiled=True),
        preferred_element_type=jnp.float32,
    )
    mix_sum = sent_and_summed(mix_terms.astype(jnp.bfloat16), "tp", 1)
    resid = (tokens.astype(jnp.float32) + mix_sum).astype(jnp.bfloat16)
    whole_ffn = gathered_copies(resid, "tp", 1)
    normed_ffn = rms_norm(whole_ffn, ffn_gain)
    gate = jnp.dot(normed_ffn, gate_full, preferred_element_type=jnp.float32)
    value = jnp.dot(normed_ffn, value_full, preferred_element_type=jnp.float32)
    gate = gate.astype(jnp.bfloat16).astype(jnp.float32)
    value = value.astype(jnp.bfloat16).astype(jnp.float32)
    gate_conv = conv_positions(gate, up_taps[0]) + up_bias[0]
    value_conv = conv_positions(value, up_taps[1]) + up_bias[1]
    hidden = (jax.nn.silu(gate_conv) * value_conv).astype(jnp.bfloat16)
    ffn_terms = jnp.dot(
        hidden, lax.all_gather(w_down, "fs", axis=1, tiled=True), preferred_element_type=jnp.float32
    )
    ffn_sum = sent_and_summed(ffn_terms.astype(jnp.bfloat16), "tp", 1)
    return (resid.astype(jnp.float32) + ffn_sum).astype(jnp.bfloat16)


def solution(mesh):
    placed = (
        P(("grp", "fs"), "tp"),
        P(),
        P("fs", "tp"),
        P("fs", "tp"),
        P("fs", "tp"),
        P(None, "tp"),
        P("tp", "fs"),
        P(),
        P("fs", "tp"),
        P("fs", "tp"),
        P(None, None, "tp"),
        P(None, "tp"),
        P("tp", "fs"),
    )
    return jax.shard_map(
        on_device, mesh=mesh, in_specs=placed, out_specs=P(("grp", "fs"), "tp"), check_vma=False
    )
```

profile of v0, /device:TPU:33, one launch (start us, length us, event | category | flops | bytes accessed | tf_op | source)
XLA Modules:
  0.0 474.6 jit_solution(4301556435789790506)
XLA Ops:
  6.6 1.4 pad_maximum_fusion.1
  8.1 1.6 pad_maximum_fusion
  9.7 1.1 copy.16
  10.8 1.3 broadcast_in_dim.4
  12.1 45.1 %all-to-all-start = ((bf16[8,384,256]{1,2,0:T(8,128)(2,1)}), bf16[8,384,256]{1,2,0:T(8,128)(2,1)S(1)}, u32[]{:S(2)}, u32[]{:S(2)}) async-start(bf16[8,384,256]{1,2,0:T(8,128)(2,1)} %broadcast_in_dim.4), calls=%async_computation | async-start | bytes 3145728 | tf_op jit(solution)/shard_map/all_to_all | solution.py:18
  57.2 52.2 %all_gather.13 = bf16[128,2048]{0,1:T(8,128)(2,1)} all-gather(bf16[128,64]{0,1:T(8,128)(2,1)S(1)} %copy-done.1), channel_id=1, replica_groups=mesh['grp'=2,'fs'=32,'tp'=8] {'fs'}, dimensions={1}, use_global_device_ids=true | all-gather | bytes 540672 | tf_op jit(solution)/shard_map/all_gather | solution.py:93
  110.3 39.8 %all-gather.4.cloned.1.call-done = bf16[2048,384]{1,0:T(8,128)(2,1)} async-done(((bf16[64,384]{1,0:T(8,128)(2,1)}), bf16[2048,384]{1,0:T(8,128)(2,1)}) %all-gather.4.cloned.1.call-update) | async-done | bytes 1572880 | tf_op jit(solution)/shard_map/all_gather | solution.py:12
  150.0 1.7 fusion.16
  151.7 1.7 fusion.15
  153.5 3.0 convolution_convert_fusion.1
  156.5 1.3 copy.25
  157.8 25.3 %all-to-all-start.1 = ((bf16[8,384,256]{2,1,0:T(8,128)(2,1)}), bf16[8,384,256]{2,1,0:T(8,128)(2,1)S(1)}, u32[]{:S(2)}, u32[]{:S(2)}) async-start(bf16[8,384,256]{2,1,0:T(8,128)(2,1)} %bitcast.59), calls=%async_computation.1 | async-start | bytes 3145728 | tf_op jit(solution)/shard_map/all_to_all | solution.py:40
  183.1 0.7 all-gather.8.cloned.1.call-update
  183.9 19.8 %all-to-all-done.1 = bf16[8,384,256]{2,1,0:T(8,128)(2,1)S(1)} async-done(((bf16[8,384,256]{2,1,0:T(8,128)(2,1)}), bf16[8,384,256]{2,1,0:T(8,128)(2,1)S(1)}, u32[]{:S(2)}, u32[]{:S(2)}) %all-to-all-start.1) | async-done | bytes 1572896 | tf_op jit(solution)/shard_map/all_to_all | solution.py:40
  204.2 1.4 broadcast_in_dim.5
  205.5 4.6 all-to-all-start.2
  210.2 20.6 %all-to-all-done.2 = bf16[8,384,256]{1,2,0:T(8,128)(2,1)S(1)} async-done(((bf16[8,384,256]{1,2,0:T(8,128)(2,1)}), bf16[8,384,256]{1,2,0:T(8,128)(2,1)S(1)}, u32[]{:S(2)}, u32[]{:S(2)}) %all-to-all-start.2) | async-done | bytes 1572896 | tf_op jit(solution)/shard_map/all_to_all | solution.py:18
  231.7 56.5 %all-gather.6.cloned.1.call-done = bf16[2048,1280]{1,0:T(8,128)(2,1)} async-done(((bf16[64,1280]{1,0:T(8,128)(2,1)}), bf16[2048,1280]{1,0:T(8,128)(2,1)}) %all-gather.6.cloned.1.call-update) | async-done | bytes 5242896 | tf_op jit(solution)/shard_map/all_gather | solution.py:12
  288.2 3.3 fusion.8
  291.6 1.4 fusion.11
  294.0 124.1 %all-gather.8.cloned.1.call-done = bf16[640,2048]{0,1:T(8,128)(2,1)} async-done(((bf16[640,64]{0,1:T(8,128)(2,1)}), bf16[640,2048]{0,1:T(8,128)(2,1)}) %all-gather.8.cloned.1.call-update) | async-done | bytes 2621456 | tf_op jit(solution)/shard_map/all_gather | solution.py:108
  418.1 3.2 convolution_convert_fusion
  421.4 45.7 %all_to_all.20 = bf16[8,384,256]{2,1,0:T(8,128)(2,1)S(1)} all-to-all(bf16[8,384,256]{2,1,0:T(8,128)(2,1)S(1)} %bitcast.61), channel_id=1, replica_groups=mesh['grp'=2,'fs'=32,'tp'=8] {'tp'}, dimensions={0} | all-to-all | bytes 3145728 | tf_op jit(solution)/shard_map/all_to_all | solution.py:40
  467.3 0.7 add_convert_fusion
  (41 shorter events, 3.8 us)
Async XLA Ops:
  6.5 143.5 %all-gather.4.cloned.1.call-start = ((), (), s32[]{:S(2)}) async-start(), calls=%async_computation.4 | async-start | bytes 1622016 | tf_op jit(solution)/shard_map/all_gather | solution.py:12
  8.0 280.2 %all-gather.6.cloned.1.call-start = ((), (), s32[]{:S(2)}) async-start(), calls=%async_computation.5 | async-start | bytes 5406720 | tf_op jit(solution)/shard_map/all_gather | solution.py:12
  12.1 45.1 %copy-start.6 = (f32[3,128]{1,0:T(4,128)S(1)}, f32[3,128]{1,0:T(4,128)}, u32[]{:S(2)}) copy-start(f32[3,128]{1,0:T(4,128)} %param.18) | copy-start | bytes 4612
  12.1 45.1 %copy-start.1 = (bf16[128,64]{0,1:T(8,128)(2,1)S(1)}, bf16[128,64]{0,1:T(8,128)(2,1)}, u32[]{:S(2)}) copy-start(bf16[128,64]{0,1:T(8,128)(2,1)} %param.19) | copy-start | bytes 49156
  12.1 97.3 %all-to-all-start = ((bf16[8,384,256]{1,2,0:T(8,128)(2,1)}), bf16[8,384,256]{1,2,0:T(8,128)(2,1)S(1)}, u32[]{:S(2)}, u32[]{:S(2)}) async-start(bf16[8,384,256]{1,2,0:T(8,128)(2,1)} %broadcast_in_dim.4), calls=%async_computation | async-start | bytes 3145728 | tf_op jit(solution)/shard_map/all_to_all | solution.py:18
  57.2 52.7 %copy-start.3 = (f32[2048]{0:T(1024)S(1)}, f32[2048]{0:T(1024)}, u32[]{:S(2)}) copy-start(f32[2048]{0:T(1024)} %param.14) | copy-start | bytes 24580
  157.8 45.9 %all-to-all-start.1 = ((bf16[8,384,256]{2,1,0:T(8,128)(2,1)}), bf16[8,384,256]{2,1,0:T(8,128)(2,1)S(1)}, u32[]{:S(2)}, u32[]{:S(2)}) async-start(bf16[8,384,256]{2,1,0:T(8,128)(2,1)} %bitcast.59), calls=%async_computation.1 | async-start | bytes 3145728 | tf_op jit(solution)/shard_map/all_to_all | solution.py:40
  183.1 20.8 %copy-start = (bf16[384,256]{1,0:T(8,128)(2,1)S(1)}, bf16[384,256]{1,0:T(8,128)(2,1)}, u32[]{:S(2)}) copy-start(bf16[384,256]{1,0:T(8,128)(2,1)} %param.13) | copy-start | bytes 589828
  183.1 235.0 %all-gather.8.cloned.1.call-start = ((), (), s32[]{:S(2)}) async-start(), calls=%async_computation.6 | async-start | bytes 2703360 | tf_op jit(solution)/shard_map/all_gather | solution.py:108
  205.5 4.6 copy-start.5
  205.5 4.6 copy-start.2
  205.5 25.3 %all-to-all-start.2 = ((bf16[8,384,256]{1,2,0:T(8,128)(2,1)}), bf16[8,384,256]{1,2,0:T(8,128)(2,1)S(1)}, u32[]{:S(2)}, u32[]{:S(2)}) async-start(bf16[8,384,256]{1,2,0:T(8,128)(2,1)} %broadcast_in_dim.5), calls=%async_computation.2 | async-start | bytes 3145728 | tf_op jit(solution)/shard_map/all_to_all | solution.py:18
  210.1 21.1 %copy-start.4 = (f32[2048]{0:T(1024)S(1)}, f32[2048]{0:T(1024)}, u32[]{:S(2)}) copy-start(f32[2048]{0:T(1024)} %param.20) | copy-start | bytes 24580
  288.2 3.4 copy-start.7
Sparse Core Ops, SparseCore 0:
  9.4 140.5 all-gather.3
  152.1 135.9 all-gather.5
  290.3 127.7 all-gather.7
where the time goes:
time: 475 us
  waiting for transfers between devices  262 us (55%)
  blocking collectives  98 us (21%)
  starting transfers between devices  75.1 us (16%)
  matrix products  14.3 us (3%)
  between operations  13.3 us (3%)
  other arithmetic  6.94 us (1%)
  local copies, waits for them, and re-layouts  5.44 us (1%)
    all_gather x1, waiting for transfers between devices, on_device(): lax.all_gather(w_down, 'fs', axis=1, tiled=True)  124 us
    all_gather x2, waiting for transfers between devices, in_one_piece(): filled = lax.all_gather(both, axis, axis=dim, tiled=True)  96.2 us
    all_gather x1, blocking collectives, on_device(): lax.all_gather(w_mix_out, 'fs', axis=1, tiled=True)  52.2 us
    all_to_all x2, starting transfers between devices, copy_for_each(): return lax.all_to_all(copies, axis, split_axis=0, concat_axis=0, tiled=True)  49.7 us
    all_to_all x1, blocking collectives, sent_and_summed(): lax.all_to_all(split_up(value, dim, devices), axis, 0, 0, tiled=True)  45.7 us
    all_to_all x1, starting transfers between devices, sent_and_summed(): lax.all_to_all(split_up(value, dim, devices), axis, 0, 0, tiled=True)  25.3 us
    all_to_all x2, waiting for transfers between devices, copy_for_each(): return lax.all_to_all(copies, axis, split_axis=0, concat_axis=0, tiled=True)  20.6 us
    all_to_all x1, waiting for transfers between devices, sent_and_summed(): lax.all_to_all(split_up(value, dim, devices), axis, 0, 0, tiled=True)  19.8 us
  transfers between devices with their start and end apart: 6, of which 5 were waited for; matrix products, arithmetic and copies ran while one was open for 4% of the time, Pallas kernels for 0%

commit v1 on v0

v1 whole, which is shorter than its diff:
```python
import functools

import jax
import jax.numpy as jnp
from jax import lax
from jax.experimental import pallas as pl
from jax.experimental.pallas import tpu as pltpu
from jax.sharding import PartitionSpec as P

SEQS_DEV = 2
LANES = 128
MESH = pl.DeviceIdType.MESH
F32, BF16 = jnp.float32, jnp.bfloat16

ONE = {"m": 2, "g": 3, "d": 1}
BOTH = {"m": 0, "g": 4, "d": 3}


def conv_positions(values, taps, length):
    row = lax.rem(lax.broadcasted_iota(jnp.int32, values.shape, 0), length)
    back1 = jnp.where(row >= 1, pltpu.roll(values, 1, 0), 0.0)
    back2 = jnp.where(row >= 2, pltpu.roll(values, 2, 0), 0.0)
    return back2 * taps[0:1] + back1 * taps[1:2] + values * taps[2:3]


def dot(a, b):
    return jnp.dot(a, b, preferred_element_type=F32)


def dot_nt(a, b):
    return lax.dot_general(a, b, (((1,), (1,)), ((), ())), preferred_element_type=F32)


def kernel(
    sizes,
    tok, mix_gain, w_sig, w_out, w_inn, mix_taps, w_mo, ffn_gain, w_gate, w_val, up_taps, up_bias, w_down,
    out,
    gm, gg, gd, act0, act1, normed, terms0, terms1, mate0, mate1, turn0, turn1, fin0, fin1, resid, hidden,
    zs_send, zs_recv, ys_send, ys_recv, ag_send, ag_recv, rs_send, rs_recv,
):
    ngrp, nz, ntp = sizes
    nx = ntp // 2
    rows, db = tok.shape
    half = rows // 2
    length = rows // SEQS_DEV
    depth = w_sig.shape[0]
    g, z, t = lax.axis_index("grp"), lax.axis_index("fs"), lax.axis_index("tp")
    y, x, c = lax.rem(g, 2), lax.div(t, 2), lax.rem(t, 2)
    pair = {"grp": g + 1 - 2 * y}
    xr, xl, x2 = lax.rem(x + 1, nx), lax.rem(x + nx - 1, nx), lax.rem(x + 2, nx)
    x_right, x_left, mate = {"tp": 2 * xr + c}, {"tp": 2 * xl + c}, {"tp": 2 * x + 1 - c}
    z_nbr = ({"fs": lax.rem(z + 1, nz)}, {"fs": lax.rem(z + nz - 1, nz)})

    def remote(src, dst, ssem, rsem, dev):
        return pltpu.make_async_remote_copy(
            src_ref=src, dst_ref=dst, send_sem=ssem, recv_sem=rsem, device_id=dev, device_id_type=MESH
        )

    sets = {"m": (gm, 0), "g": (gg, 1), "d": (gd, 2)}
    steps = (nz // 2, (nz - 1) // 2)

    def piece(ref, first, count, origin):
        return ref.at[pl.ds(first, count), pl.ds(pl.multiple_of(origin * depth, depth), depth), :]

    def origin_of(way, s):
        return lax.rem(z + (nz - s if way == 0 else s), nz)

    def z_copy(name, way, s):
        ref, k = sets[name]
        part = piece(ref, ONE[name] * y, ONE[name] + BOTH[name], origin_of(way, s))
        return remote(part, part, zs_send.at[k, way, s], zs_recv.at[k, way, s], z_nbr[way])

    def z_arrive(name, way, s):
        ref, k = sets[name]
        part = piece(ref, ONE[name] * y, ONE[name] + BOTH[name], origin_of(way, s + 1))
        remote(part, part, zs_send.at[k, way, s], zs_recv.at[k, way, s], z_nbr[way]).wait_recv()

    def y_copy(name, way, s):
        ref, k = sets[name]
        part = piece(ref, (ONE[name] + BOTH[name]) * y, ONE[name], origin_of(way, s + 1))
        return remote(part, part, ys_send.at[k, way, s], ys_recv.at[k], pair)

    def z_open(name):
        for way in (0, 1):
            z_copy(name, way, 0).start()

    def z_step(name, s):
        for way in (0, 1):
            def go(way=way):
                z_arrive(name, way, s)
                pl.when(s + 1 < steps[way])(lambda: z_copy(name, way, s + 1).start())
                y_copy(name, way, s).start()
            pl.when(s < steps[way])(go)

    def z_steps(name, lo, hi):
        def body(s, _):
            z_step(name, s)
            return 0
        lax.fori_loop(lo, hi, body, 0)

    def y_arrive(name):
        ref, k = sets[name]
        part = ref.at[pl.ds(0, ONE[name]), pl.ds(0, (nz - 1) * depth), :]
        remote(part, part, ys_send.at[k, 0, 0], ys_recv.at[k], pair).wait_recv()

    def ag_copies(act, k):
        own, lft, rgt, far = act.at[t], act.at[2 * xl + c], act.at[2 * xr + c], act.at[2 * x2 + c]
        top, bot = pl.ds(0, half), pl.ds(half, half)
        plan = (
            (own, x_right), (own, x_left), (own, mate),
            (lft.at[top], x_right), (lft, mate), (rgt.at[bot], x_left), (rgt, mate),
            (far.at[top], mate), (far.at[bot], mate),
        )
        return [remote(r, r, ag_send.at[k, i], ag_recv.at[k, i], dev) for i, (r, dev) in enumerate(plan)]

    def ag_lands(act, k):
        o = 1 - c
        top, bot = pl.ds(0, half), pl.ds(half, half)
        far, ofar = act.at[2 * x2 + c], act.at[2 * x2 + o]
        plan = (
            act.at[2 * xl + c], act.at[2 * xr + c], act.at[2 * x + o],
            far.at[top], act.at[2 * xl + o], far.at[bot], act.at[2 * xr + o],
            ofar.at[top], ofar.at[bot],
        )
        return [remote(r, r, ag_send.at[k, i], ag_recv.at[k, i], mate) for i, r in enumerate(plan)]

    def rs_copies(k, terms, mt, turn, fin):
        top, bot = pl.ds(0, half), pl.ds(half, half)
        plan = [(terms.at[2 * v + 1 - c], mt.at[v], mate) for v in (x2, xr, xl, x)]
        plan += [
            (terms.at[2 * x2 + c, top], turn.at[0], x_right),
            (terms.at[2 * x2 + c, bot], turn.at[1], x_left),
            (terms.at[2 * xr + c, bot], fin.at[0, bot], x_right),
            (terms.at[2 * xl + c, top], fin.at[1, top], x_left),
            (terms.at[2 * xr + c, top], fin.at[0, top], x_right),
            (terms.at[2 * xl + c, bot], fin.at[1, bot], x_left),
        ]
        return [remote(s, d, rs_send.at[k, i], rs_recv.at[k, i], dev) for i, (s, d, dev) in enumerate(plan)]

    def reduce_scatter(k, term_of, terms, mt, turn, fin, between):
        copies = rs_copies(k, terms, mt, turn, fin)
        top, bot = pl.ds(0, half), pl.ds(half, half)
        for i, v in enumerate((x2, xr, xl, x)):
            terms[2 * v + 1 - c] = term_of(2 * v + 1 - c).astype(BF16)
            copies[i].start()
            terms[2 * v + c] = term_of(2 * v + c).astype(BF16)

        def join(i, v):
            copies[i].wait_recv()
            terms[2 * v + c] = (terms[2 * v + c].astype(F32) + mt[v].astype(F32)).astype(BF16)

        join(0, x2)
        copies[4].start()
        copies[5].start()
        join(1, xr)
        copies[6].start()
        join(2, xl)
        copies[7].start()
        between()
        copies[4].wait_recv()
        terms[2 * xr + c, top] = (terms[2 * xr + c, top].astype(F32) + turn[0].astype(F32)).astype(BF16)
        copies[8].start()
        copies[5].wait_recv()
        terms[2 * xl + c, bot] = (terms[2 * xl + c, bot].astype(F32) + turn[1].astype(F32)).astype(BF16)
        copies[9].start()
        copies[3].wait_recv()
        total = terms[2 * x + c].astype(F32) + mt[x].astype(F32)
        for i in (6, 7, 8, 9):
            copies[i].wait_recv()
        total += fin[0].astype(F32) + fin[1].astype(F32)
        return total, copies

    def norm(act, gain):
        total = jnp.zeros((rows, 1), F32)
        for b in range(ntp):
            v = act[b].astype(F32)
            total += jnp.sum(v * v, axis=1, keepdims=True)
        scale = lax.rsqrt(total / (ntp * db) + 1e-06)
        for b in range(ntp):
            cols = slice(b * db, (b + 1) * db)
            normed[:, cols] = (act[b].astype(F32) * scale * gain[:, cols]).astype(BF16)

    mine = pl.ds(pl.multiple_of(z * depth, depth), depth)
    eye = (
        lax.broadcasted_iota(jnp.int32, (depth, depth), 0) == lax.broadcasted_iota(jnp.int32, (depth, depth), 1)
    ).astype(BF16)
    for k, ref in enumerate((w_sig, w_out, w_inn)):
        gm[k, mine, :] = ref[...]
    gm[3, mine, :] = dot_nt(eye, w_mo[...]).astype(BF16)
    act0[t] = tok[...]
    nf = w_gate.shape[1] // LANES
    for b in range(nf):
        cols = slice(b * LANES, (b + 1) * LANES)
        gg[b, mine, :] = w_gate[:, cols]
        gg[nf + b, mine, :] = w_val[:, cols]
        gd[b, mine, :] = dot_nt(eye, w_down[cols, :]).astype(BF16)

    barrier = pltpu.get_barrier_semaphore()
    friends = (x_right, x_left, mate, *z_nbr, pair)
    for dev in friends:
        pl.semaphore_signal(barrier, inc=1, device_id=dev, device_id_type=MESH)
    pl.semaphore_wait(barrier, len(friends))

    z_open("m")
    ag0, land0 = ag_copies(act0, 0), ag_lands(act0, 0)
    for i in (0, 1, 2):
        ag0[i].start()
    z_open("g")

    z_step("m", 0)
    land0[0].wait_recv()
    ag0[3].start()
    ag0[4].start()
    land0[1].wait_recv()
    ag0[5].start()
    ag0[6].start()
    z_step("m", 1)
    z_step("g", 0)
    z_step("m", 2)
    land0[3].wait_recv()
    ag0[7].start()
    land0[5].wait_recv()
    ag0[8].start()
    z_step("m", 3)
    z_step("g", 1)
    z_step("m", 4)
    for i in (2, 4, 6, 7, 8):
        land0[i].wait_recv()
    norm(act0, mix_gain)

    last = steps[0]

    def pace(i, _):
        z_step("m", 2 * i + 1)
        z_step("g", i)
        z_step("m", 2 * i + 2)
        return 0

    lax.fori_loop(2, (last - 1) // 2, pace, 0)
    z_step("m", last - 1)
    done_g = (last - 1) // 2
    z_step("g", done_g)
    y_arrive("m")

    three = dot(normed[...], jnp.concatenate([gm[0], gm[1], gm[2]], axis=1)).astype(BF16).astype(F32)
    signal, outer, inner = (three[:, k * LANES : (k + 1) * LANES] for k in range(3))
    mixed = (outer * conv_positions(inner * signal, mix_taps[...], length)).astype(BF16)
    z_step("g", done_g + 1)

    def mix_term(b):
        return dot_nt(mixed, gm[3, pl.ds(pl.multiple_of(b * db, db), db), :])

    total, rs0 = reduce_scatter(0, mix_term, terms0, mate0, turn0, fin0, lambda: z_steps("g", done_g + 2, done_g + 4))
    stream = (tok[...].astype(F32) + total).astype(BF16)
    resid[...] = stream
    act1[t] = stream
    ag1, land1 = ag_copies(act1, 1), ag_lands(act1, 1)
    for i in (0, 1, 2):
        ag1[i].start()
    z_open("d")
    z_step("g", done_g + 4)
    land1[0].wait_recv()
    ag1[3].start()
    ag1[4].start()
    land1[1].wait_recv()
    ag1[5].start()
    ag1[6].start()
    z_step("g", done_g + 5)
    land1[3].wait_recv()
    ag1[7].start()
    land1[5].wait_recv()
    ag1[8].start()
    for i in (2, 4, 6, 7, 8):
        land1[i].wait_recv()
    norm(act1, ffn_gain)
    z_steps("g", done_g + 6, last)

    def d_pace(s, _):
        z_step("d", s)
        return 0

    lax.fori_loop(0, 2, d_pace, 0)
    y_arrive("g")
    for b in range(nf):
        both = dot(normed[...], jnp.concatenate([gg[b], gg[nf + b]], axis=1)).astype(BF16).astype(F32)
        cols = slice(b * LANES, (b + 1) * LANES)
        gate = conv_positions(both[:, :LANES], up_taps[0, :, cols], length) + up_bias[0:1, cols]
        value = conv_positions(both[:, LANES:], up_taps[1, :, cols], length) + up_bias[1:2, cols]
        hidden[:, cols] = (gate / (1.0 + jnp.exp(-gate)) * value).astype(BF16)
        z_step("d", 2 + b)
    lax.fori_loop(2 + nf, last, d_pace, 0)
    y_arrive("d")

    def ffn_term(b):
        at = pl.ds(pl.multiple_of(b * db, db), db)
        return dot_nt(hidden[...], jnp.concatenate([gd[i, at, :] for i in range(nf)], axis=1))

    total, rs1 = reduce_scatter(1, ffn_term, terms1, mate1, turn1, fin1, lambda: None)
    out[...] = (resid[...].astype(F32) + total).astype(BF16)

    for copy in (*ag0, *ag1, *rs0, *rs1):
        copy.wait_send()
    for name in sets:
        for way in (0, 1):
            def drain(s, _, name=name, way=way):
                z_copy(name, way, s).wait_send()
                y_copy(name, way, s).wait_send()
                return 0
            lax.fori_loop(0, steps[way], drain, 0)


def on_device(sizes, tokens, mix_gain, w_signal, w_outer, w_inner, mix_taps, w_mix_out, ffn_gain, w_gate, w_value, up_taps, up_bias, w_down):
    rows, db = tokens.shape
    ntp, nz = sizes[2], sizes[1]
    d = ntp * db
    nf = w_gate.shape[1] // LANES
    half = rows // 2
    vmem, dma = pltpu.VMEM, pltpu.SemaphoreType.DMA
    act = vmem((ntp, rows, db), BF16)
    mt, turn, fin = vmem((ntp // 2, rows, db), BF16), vmem((2, half, db), BF16), vmem((2, rows, db), BF16)
    scratch = [
        vmem((4, d, LANES), BF16), vmem((2 * nf, d, LANES), BF16), vmem((nf, d, LANES), BF16),
        act, act, vmem((rows, d), BF16), act, act, mt, mt, turn, turn, fin, fin,
        vmem((rows, db), BF16), vmem((rows, nf * LANES), BF16),
        dma((3, 2, nz // 2)), dma((3, 2, nz // 2)), dma((3, 2, nz // 2)), dma((3,)),
        dma((2, 9)), dma((2, 9)), dma((2, 10)), dma((2, 10)),
    ]
    args = (
        tokens, mix_gain.reshape(1, d), w_signal, w_outer, w_inner, mix_taps, w_mix_out, ffn_gain.reshape(1, d),
        w_gate, w_value, up_taps, up_bias, w_down,
    )
    return pl.pallas_call(
        functools.partial(kernel, sizes),
        out_shape=jax.ShapeDtypeStruct((rows, db), BF16),
        in_specs=[pl.BlockSpec(memory_space=vmem)] * len(args),
        out_specs=pl.BlockSpec(memory_space=vmem),
        scratch_shapes=scratch,
        compiler_params=pltpu.CompilerParams(
            collective_id=0, has_side_effects=True, vmem_limit_bytes=60 * 1024 * 1024
        ),
        name="layer",
    )(*args)


def solution(mesh):
    sizes = (mesh.shape["grp"], mesh.shape["fs"], mesh.shape["tp"])
    placed = (
        P(("grp", "fs"), "tp"), P(), P("fs", "tp"), P("fs", "tp"), P("fs", "tp"), P(None, "tp"), P("tp", "fs"), P(),
        P("fs", "tp"), P("fs", "tp"), P(None, None, "tp"), P(None, "tp"), P("tp", "fs"),
    )
    return jax.shard_map(
        functools.partial(on_device, sizes),
        mesh=mesh, in_specs=placed, out_specs=P(("grp", "fs"), "tp"), check_vma=False,
    )
```

time: 475 us -> 215 us (0.45)
  waiting for transfers between devices: 262 us -> 0 us
  Pallas kernels: 0 us -> 209 us
  blocking collectives: 98 us -> 0 us
  starting transfers between devices: 75.1 us -> 0 us
  matrix products: 14.3 us -> 0 us
  between operations: 13.3 us -> 0.01 us
  other arithmetic: 6.94 us -> 0 us
    all_gather x3 -> x0, waiting for transfers between devices: 220 us -> none  [the longest x1 124 us: on_device(): lax.all_gather(w_down, 'fs', axis=1, tiled=True)]
    pallas_call x0 -> x1, Pallas kernels: none -> 209 us  [on_device(): pl.pallas_call(functools.partial(kernel, sizes), out_shape=jax.ShapeDtype...]
    all_to_all x3 -> x0, starting transfers between devices: 75 us -> none  [the longest x2 49.7 us: copy_for_each(): return lax.all_to_all(copies, axis, split_axis=0, concat_axis=0, tiled=True)]
    all_gather x1 -> x0, blocking collectives: 52.2 us -> none  [on_device(): lax.all_gather(w_mix_out, 'fs', axis=1, tiled=True)]
    all_to_all x1 -> x0, blocking collectives: 45.7 us -> none  [sent_and_summed(): lax.all_to_all(split_up(value, dim, devices), axis, 0, 0, tiled=True)]
    all_to_all x3 -> x0, waiting for transfers between devices: 40.4 us -> none  [the longest x2 20.6 us: copy_for_each(): return lax.all_to_all(copies, axis, split_axis=0, concat_axis=0, tiled=True)]
    dot_general x6 -> x0, matrix products: 14.3 us -> none  [the longest x1 3.31 us: on_device(): gate = jnp.dot(normed_ffn, gate_full, preferred_element_type=jnp.float32)]
  transfers between devices with their start and end apart: 6 -> 0, of which waited for: 5 -> 0; matrix products, arithmetic and copies ran while one was open for 4% -> 0% of each run, Pallas kernels for 0% -> 0%
where the time goes in v1:
time: 215 us; the launch traced here: 214 us
  Pallas kernels  209 us (97%)
  local copies, waits for them, and re-layouts  5.22 us (2%)
    pallas_call x1, Pallas kernels, on_device(): pl.pallas_call(functools.partial(kernel, sizes), out_shape=jax.ShapeDtype...  209 us
    unnamed x6, local copies, waits for them, and re-layouts  5.22 us

profile of v1, /device:TPU:33, one launch (start us, length us, event | category | flops | bytes accessed | tf_op | source)
XLA Modules:
  0.0 214.1 jit_solution(6580914214646516613)
XLA Ops:
  0.0 0.0 copy-start
  0.0 1.4 copy.15.up_taps
  1.4 1.4 copy.14.w_mo
  2.8 0.0 copy-done
  2.8 0.8 copy.16.w_down
  3.6 208.9 %layer.1 = bf16[384,256]{1,0:T(8,128)(2,1)} custom-call(bf16[384,256]{1,0:T(8,128)(2,1)} %tok.1, f32[1,2048]{1,0:T(1,128)} %bitcast.2, bf16[64,128]{1,0:T(8,128)(2,1)} %w_sig.1, bf16[64,128]{1,0:T(8,128)(2,1)} %w_out.1, bf16[64,128]{1,0:T(8,128)(2,1)} %w_inn.1, f32[3,128]{1,0:T(4,128)} %mix_taps.1, bf16[128,64]{1,0:T(8,128)(2,1)} %copy.14.w_mo, ...), custom_call_target="tpu_custom_call" | custom-call | tf_op jit(solution)/shard_map/layer/pallas_call | solution.py:332
  212.5 1.6 copy.18
Async XLA Ops:
  0.0 2.8 %copy-start = (bf16[640,64]{0,1:T(8,128)(2,1)S(1)}, bf16[640,64]{0,1:T(8,128)(2,1)}, u32[]{:S(2)}) copy-start(bf16[640,64]{0,1:T(8,128)(2,1)} %param.25) | copy-start | bytes 245764

commit v2 on v1

v2 whole, which is shorter than its diff:
```python
import functools

import jax
import jax.numpy as jnp
from jax import lax
from jax.experimental import pallas as pl
from jax.experimental.pallas import tpu as pltpu
from jax.sharding import PartitionSpec as P

SEQS_DEV = 2
LANES = 128
MESH = pl.DeviceIdType.MESH
F32, BF16 = jnp.float32, jnp.bfloat16

ONE = {"m": 2, "g": 4, "d": 1}
BOTH = {"m": 0, "g": 2, "d": 3}
UP_M, UP_F = 16, 16
MIXER_AT = 8


def conv_positions(values, taps, length):
    row = lax.rem(lax.broadcasted_iota(jnp.int32, values.shape, 0), length)
    back1 = jnp.where(row >= 1, pltpu.roll(values, 1, 0), 0.0)
    back2 = jnp.where(row >= 2, pltpu.roll(values, 2, 0), 0.0)
    return back2 * taps[0:1] + back1 * taps[1:2] + values * taps[2:3]


def dot(a, b):
    return jnp.dot(a, b, preferred_element_type=F32)


def dot_nt(a, b):
    return lax.dot_general(a, b, (((1,), (1,)), ((), ())), preferred_element_type=F32)


def kernel(
    sizes,
    tok, mix_gain, w_sig, w_out, w_inn, mix_taps, w_mo, ffn_gain, w_gate, w_val, up_taps, up_bias, w_down,
    out,
    gm, gg, gd, act0, act1, normed, terms0, terms1, mate0, mate1, turn0, turn1, fin0, fin1, resid, hidden,
    m_recv, g_recv, d_recv, ring_send, y_send, y_recv, push_send, push_recv, own_send, own_recv,
    ag_send, ag_recv, rs_send, rs_recv,
):
    ngrp, nz, ntp = sizes
    nx = ntp // 2
    rows, db = tok.shape
    half = rows // 2
    length = rows // SEQS_DEV
    depth = w_sig.shape[0]
    nf = w_gate.shape[1] // LANES
    g, z, t = lax.axis_index("grp"), lax.axis_index("fs"), lax.axis_index("tp")
    y, x, c = lax.rem(g, 2), lax.div(t, 2), lax.rem(t, 2)
    other = g + 1 - 2 * y
    xr, xl, x2 = lax.rem(x + 1, nx), lax.rem(x + nx - 1, nx), lax.rem(x + 2, nx)
    x_right, x_left, mate = {"tp": 2 * xr + c}, {"tp": 2 * xl + c}, {"tp": 2 * x + 1 - c}
    def remote(src, dst, ssem, rsem, dev):
        return pltpu.make_async_remote_copy(
            src_ref=src, dst_ref=dst, send_sem=ssem, recv_sem=rsem, device_id=dev, device_id_type=MESH
        )

    refs = {"m": gm, "g": gg, "d": gd}
    index = {"m": 0, "g": 1, "d": 2}
    most = {"m": (UP_M, nz - 1 - UP_M), "g": (UP_F, nz - 1 - UP_F), "d": (UP_F, nz - 1 - UP_F)}
    recv_of = {"m": m_recv, "g": g_recv, "d": d_recv}
    is_m, is_f = c == 1, c == 0

    def z_part(name, col, origin):
        at = pl.ds(pl.multiple_of(origin * depth, depth), depth)
        return refs[name].at[col, pl.ds(ONE[name] * y, ONE[name] + BOTH[name]), at, :]

    def y_part(name, col, origin):
        at = pl.ds(pl.multiple_of(origin * depth, depth), depth)
        return refs[name].at[col, pl.ds((ONE[name] + BOTH[name]) * y, ONE[name]), at, :]

    def fs_at(k):
        return lax.rem(z + nz + k, nz)

    def origin_of(way, dist):
        return fs_at(-dist if way == 0 else dist)

    def send(name, col, way, dist, hops):
        part = z_part(name, col, origin_of(way, dist))
        to = {"fs": fs_at(hops if way == 0 else -hops)}
        remote(part, part, ring_send.at[index[name]], recv_of[name].at[col, way, dist + hops - 1], to).start()

    def landed(name, col, way, dist):
        part = z_part(name, col, origin_of(way, dist))
        sem = recv_of[name].at[col, way, dist - 1]
        remote(part, part, ring_send.at[index[name]], sem, mate).wait_recv()

    def spread(name, col, way, dist):
        k, origin = index[name], origin_of(way, dist)
        part, cross = z_part(name, col, origin), y_part(name, col, origin)
        remote(cross, cross, y_send.at[k], y_recv.at[k], {"grp": other, "tp": 2 * x + col}).start()
        if col != (1 if name == "m" else 0):
            remote(part, part, push_send.at[k], push_recv.at[k], mate).start()

    def mixer_step(way, first, upto):
        for dist in (first, first + 1):
            @pl.when(dist <= upto)
            def _(dist=dist):
                for col in (0, 1):
                    landed("m", col, way, dist)
                    pl.when(dist + 2 <= upto)(lambda: send("m", col, way, dist, 2))
                for col in (0, 1):
                    spread("m", col, way, dist)

    def bulk_step(i):
        dist = i + 1
        for col in (0, 1):
            for name in ("g", "d"):
                for way in (0, 1):
                    @pl.when(dist <= most[name][way])
                    def _(way=way):
                        landed(name, col, way, dist)
                        pl.when(dist + 1 <= most[name][way])(lambda: send(name, col, way, dist, 1))
                        spread(name, col, way, dist)

    def open_ring(kind, cols):
        for col in cols:
            for way in (0, 1):
                if kind == "m":
                    send("m", col, way, 0, 1)
                    send("m", col, way, 0, 2)
                else:
                    for name in ("g", "d"):
                        send(name, col, way, 0, 1)

    mixer_end = (max(most["m"]) + 1) // 2
    bulk_end = max(most["g"])

    def mixer_steps(lo, hi):
        def body(i, _):
            for way in (0, 1):
                mixer_step(way, 2 * i + 1, most["m"][way])
            return 0

        lax.fori_loop(lo, jnp.where(is_m, hi, lo), body, 0)

    def bulk_steps(lo, hi):
        hi = min(hi, bulk_end)
        lax.fori_loop(lo, jnp.where(is_f, hi, lo), lambda i, _: (bulk_step(i), 0)[1], 0)
        return hi

    def arrive(name):
        k, span = index[name], pl.ds(0, (nz - 1) * depth)
        part = refs[name].at[0, pl.ds(0, ONE[name]), span, :]
        remote(part, part, y_send.at[k], y_recv.at[k], mate).wait_recv()
        rest = refs[name].at[0, pl.ds(0, ONE[name] + BOTH[name]), span, :]
        pl.when(is_f if name == "m" else is_m)(
            lambda: remote(rest, rest, push_send.at[k], push_recv.at[k], mate).wait_recv()
        )

    def ag_copies(act, k):
        own, lft, rgt, far = act.at[t], act.at[2 * xl + c], act.at[2 * xr + c], act.at[2 * x2 + c]
        top, bot = pl.ds(0, half), pl.ds(half, half)
        plan = (
            (own, x_right), (own, x_left), (own, mate),
            (lft.at[top], x_right), (lft, mate), (rgt.at[bot], x_left), (rgt, mate),
            (far.at[top], mate), (far.at[bot], mate),
        )
        return [remote(r, r, ag_send.at[k, i], ag_recv.at[k, i], dev) for i, (r, dev) in enumerate(plan)]

    def ag_lands(act, k):
        o = 1 - c
        top, bot = pl.ds(0, half), pl.ds(half, half)
        far, ofar = act.at[2 * x2 + c], act.at[2 * x2 + o]
        plan = (
            act.at[2 * xl + c], act.at[2 * xr + c], act.at[2 * x + o],
            far.at[top], act.at[2 * xl + o], far.at[bot], act.at[2 * xr + o],
            ofar.at[top], ofar.at[bot],
        )
        return [remote(r, r, ag_send.at[k, i], ag_recv.at[k, i], mate) for i, r in enumerate(plan)]

    def rs_copies(k, terms, mt, turn, fin):
        top, bot = pl.ds(0, half), pl.ds(half, half)
        plan = [(terms.at[2 * v + 1 - c], mt.at[v], mate) for v in (x2, xr, xl, x)]
        plan += [
            (terms.at[2 * x2 + c, top], turn.at[0], x_right),
            (terms.at[2 * x2 + c, bot], turn.at[1], x_left),
            (terms.at[2 * xr + c, bot], fin.at[0, bot], x_right),
            (terms.at[2 * xl + c, top], fin.at[1, top], x_left),
            (terms.at[2 * xr + c, top], fin.at[0, top], x_right),
            (terms.at[2 * xl + c, bot], fin.at[1, bot], x_left),
        ]
        return [remote(s, d, rs_send.at[k, i], rs_recv.at[k, i], dev) for i, (s, d, dev) in enumerate(plan)]

    def reduce_scatter(k, term_of, terms, mt, turn, fin, between):
        copies = rs_copies(k, terms, mt, turn, fin)
        top, bot = pl.ds(0, half), pl.ds(half, half)
        for i, v in enumerate((x2, xr, xl, x)):
            terms[2 * v + 1 - c] = term_of(2 * v + 1 - c).astype(BF16)
            copies[i].start()
            terms[2 * v + c] = term_of(2 * v + c).astype(BF16)

        def join(i, v):
            copies[i].wait_recv()
            terms[2 * v + c] = (terms[2 * v + c].astype(F32) + mt[v].astype(F32)).astype(BF16)

        join(0, x2)
        copies[4].start()
        copies[5].start()
        join(1, xr)
        copies[6].start()
        join(2, xl)
        copies[7].start()
        between()
        copies[4].wait_recv()
        terms[2 * xr + c, top] = (terms[2 * xr + c, top].astype(F32) + turn[0].astype(F32)).astype(BF16)
        copies[8].start()
        copies[5].wait_recv()
        terms[2 * xl + c, bot] = (terms[2 * xl + c, bot].astype(F32) + turn[1].astype(F32)).astype(BF16)
        copies[9].start()
        copies[3].wait_recv()
        total = terms[2 * x + c].astype(F32) + mt[x].astype(F32)
        for i in (6, 7, 8, 9):
            copies[i].wait_recv()
        total += fin[0].astype(F32) + fin[1].astype(F32)
        return total, copies

    def norm(act, gain):
        total = jnp.zeros((rows, 1), F32)
        for b in range(ntp):
            v = act[b].astype(F32)
            total += jnp.sum(v * v, axis=1, keepdims=True)
        scale = lax.rsqrt(total / (ntp * db) + 1e-06)
        for b in range(ntp):
            cols = slice(b * db, (b + 1) * db)
            normed[:, cols] = (act[b].astype(F32) * scale * gain[:, cols]).astype(BF16)

    mine = pl.ds(pl.multiple_of(z * depth, depth), depth)
    for k, ref in enumerate((w_sig, w_out, w_inn, w_mo)):
        gm[c, k, mine, :] = ref[...]
    act0[t] = tok[...]
    for b in range(nf):
        cols = slice(b * LANES, (b + 1) * LANES)
        gg[c, b, mine, :] = w_gate[:, cols]
        gg[c, nf + b, mine, :] = w_val[:, cols]
        gd[c, b, mine, :] = w_down[:, cols]

    barrier = pltpu.get_barrier_semaphore()
    near = (x_right, x_left, mate, {"grp": other}, {"grp": other, "tp": 2 * x + 1 - c})
    below = [{"fs": lax.rem(z + nz - k, nz)} for k in (1, 2)]
    above = [{"fs": lax.rem(z + k, nz)} for k in (1, 2)]
    for dev in (*below, *above, *near):
        pl.semaphore_signal(barrier, inc=1, device_id=dev, device_id_type=MESH)
    pl.semaphore_wait(barrier, len(near) + len(above) + len(below))

    names = ("m", "g", "d")
    to_mate = []
    for i, name in enumerate(names):
        p = z_part(name, 0 if name == "m" else 1, z)
        to_mate.append(remote(p, p, own_send.at[i], own_recv.at[i], mate))
    ag0, land0 = ag_copies(act0, 0), ag_lands(act0, 0)

    @pl.when(is_f)
    def _():
        to_mate[0].start()
        open_ring("f", (0,))

    @pl.when(is_m)
    def _():
        to_mate[1].start()
        to_mate[2].start()
        open_ring("m", (1,))
        to_mate[0].wait_recv()
        open_ring("m", (0,))

    for i in (0, 1, 2):
        ag0[i].start()

    @pl.when(is_f)
    def _():
        to_mate[1].wait_recv()
        to_mate[2].wait_recv()
        open_ring("f", (1,))

    mixer_steps(0, 1)
    bulk_steps(0, 1)
    land0[0].wait_recv()
    ag0[3].start()
    ag0[4].start()
    land0[1].wait_recv()
    ag0[5].start()
    ag0[6].start()
    mixer_steps(1, 2)
    bulk_steps(1, 2)
    land0[3].wait_recv()
    ag0[7].start()
    land0[5].wait_recv()
    ag0[8].start()
    for i in (2, 4, 6, 7, 8):
        land0[i].wait_recv()
    norm(act0, mix_gain)
    mixer_steps(2, mixer_end)
    done = bulk_steps(2, MIXER_AT)
    arrive("m")

    wide = jnp.concatenate([gm[c, 0], gm[c, 1], gm[c, 2]], axis=1)
    three = dot(normed[...], wide).astype(BF16).astype(F32)
    signal, outer, inner = (three[:, k * LANES : (k + 1) * LANES] for k in range(3))
    mixed = (outer * conv_positions(inner * signal, mix_taps[...], length)).astype(BF16)

    done = bulk_steps(done, done + 1)

    def mix_term(b):
        return dot_nt(mixed, gm[c, 3, pl.ds(pl.multiple_of(b * db, db), db), :])

    total, rs0 = reduce_scatter(0, mix_term, terms0, mate0, turn0, fin0, lambda: None)
    stream = (tok[...].astype(F32) + total).astype(BF16)
    resid[...] = stream
    act1[t] = stream
    ag1, land1 = ag_copies(act1, 1), ag_lands(act1, 1)
    for i in (0, 1, 2):
        ag1[i].start()
    done = bulk_steps(done, done + 2)
    land1[0].wait_recv()
    ag1[3].start()
    ag1[4].start()
    land1[1].wait_recv()
    ag1[5].start()
    ag1[6].start()
    done = bulk_steps(done, done + 1)
    land1[3].wait_recv()
    ag1[7].start()
    land1[5].wait_recv()
    ag1[8].start()
    done = bulk_steps(done, done + 1)
    for i in (2, 4, 6, 7, 8):
        land1[i].wait_recv()
    norm(act1, ffn_gain)
    bulk_steps(done, bulk_end)

    arrive("g")
    for b in range(nf):
        both = dot(normed[...], jnp.concatenate([gg[c, b], gg[c, nf + b]], axis=1)).astype(BF16).astype(F32)
        cols = slice(b * LANES, (b + 1) * LANES)
        gate = conv_positions(both[:, :LANES], up_taps[:, 0, cols], length) + up_bias[0:1, cols]
        value = conv_positions(both[:, LANES:], up_taps[:, 1, cols], length) + up_bias[1:2, cols]
        hidden[:, cols] = (gate / (1.0 + jnp.exp(-gate)) * value).astype(BF16)
    arrive("d")

    def ffn_term(b):
        at = pl.ds(pl.multiple_of(b * db, db), db)
        return dot_nt(hidden[...], jnp.concatenate([gd[c, i, at, :] for i in range(nf)], axis=1))

    total, rs1 = reduce_scatter(1, ffn_term, terms1, mate1, turn1, fin1, lambda: None)
    out[...] = (resid[...].astype(F32) + total).astype(BF16)

    for copy in (*ag0, *ag1, *rs0, *rs1):
        copy.wait_send()

    def drain(name):
        k, n, span = index[name], ONE[name] + BOTH[name], pl.ds(0, (nz - 1) * depth)
        sent = refs[name].at[:, pl.ds(0, n), span, :]
        remote(sent, sent, ring_send.at[k], own_recv.at[0], mate).wait_send()
        crossed = refs[name].at[:, pl.ds(0, ONE[name]), span, :]
        remote(crossed, crossed, y_send.at[k], own_recv.at[0], mate).wait_send()
        pushed = refs[name].at[0, pl.ds(0, n), span, :]
        remote(pushed, pushed, push_send.at[k], own_recv.at[0], mate).wait_send()

    @pl.when(is_f)
    def _():
        to_mate[0].wait_send()
        drain("g")
        drain("d")

    @pl.when(is_m)
    def _():
        to_mate[1].wait_send()
        to_mate[2].wait_send()
        drain("m")


def on_device(sizes, tokens, mix_gain, w_signal, w_outer, w_inner, mix_taps, w_mix_out, ffn_gain, w_gate, w_value, up_taps, up_bias, w_down):
    rows, db = tokens.shape
    ntp, nz = sizes[2], sizes[1]
    d = ntp * db
    nf = w_gate.shape[1] // LANES
    half = rows // 2
    vmem, dma = pltpu.VMEM, pltpu.SemaphoreType.DMA
    act = vmem((ntp, rows, db), BF16)
    mt, turn, fin = vmem((ntp // 2, rows, db), BF16), vmem((2, half, db), BF16), vmem((2, rows, db), BF16)
    scratch = [
        vmem((2, 4, d, LANES), BF16), vmem((2, 2 * nf, d, LANES), BF16), vmem((2, nf, d, LANES), BF16),
        act, act, vmem((rows, d), BF16), act, act, mt, mt, turn, turn, fin, fin,
        vmem((rows, db), BF16), vmem((rows, nf * LANES), BF16),
        dma((2, 2, nz)), dma((2, 2, nz)), dma((2, 2, nz)), dma((3,)), dma((3,)), dma((3,)), dma((3,)), dma((3,)),
        dma((3,)), dma((3,)), dma((2, 9)), dma((2, 9)), dma((2, 10)), dma((2, 10)),
    ]
    args = (
        tokens, mix_gain.reshape(1, d), w_signal, w_outer, w_inner, mix_taps, w_mix_out.T, ffn_gain.reshape(1, d),
        w_gate, w_value, jnp.transpose(up_taps, (1, 0, 2)), up_bias, w_down.T,
    )
    return pl.pallas_call(
        functools.partial(kernel, sizes),
        out_shape=jax.ShapeDtypeStruct((rows, db), BF16),
        in_specs=[pl.BlockSpec(memory_space=vmem)] * len(args),
        out_specs=pl.BlockSpec(memory_space=vmem),
        scratch_shapes=scratch,
        compiler_params=pltpu.CompilerParams(
            collective_id=0, has_side_effects=True, vmem_limit_bytes=60 * 1024 * 1024
        ),
        name="layer",
    )(*args)


def solution(mesh):
    sizes = (mesh.shape["grp"], mesh.shape["fs"], mesh.shape["tp"])
    placed = (
        P(("grp", "fs"), "tp"), P(), P("fs", "tp"), P("fs", "tp"), P("fs", "tp"), P(None, "tp"), P("tp", "fs"), P(),
        P("fs", "tp"), P("fs", "tp"), P(None, None, "tp"), P(None, "tp"), P("tp", "fs"),
    )
    return jax.shard_map(
        functools.partial(on_device, sizes),
        mesh=mesh, in_specs=placed, out_specs=P(("grp", "fs"), "tp"), check_vma=False,
    )
```

time: 215 us -> 166 us (0.77)
  Pallas kernels: 209 us -> 164 us
  local copies, waits for them, and re-layouts: 5.22 us -> 1.62 us
    pallas_call x1, Pallas kernels: 209 us -> 164 us  [on_device(): pl.pallas_call(functools.partial(kernel, sizes), out_shape=jax.ShapeDtype...]
    unnamed x6 -> x1, local copies, waits for them, and re-layouts: 5.22 us -> 1.62 us
where the time goes in v2:
time: 166 us
  Pallas kernels  164 us (99%)
    pallas_call x1, Pallas kernels, on_device(): pl.pallas_call(functools.partial(kernel, sizes), out_shape=jax.ShapeDtype...  164 us

profile of v2, /device:TPU:33, one launch (start us, length us, event | category | flops | bytes accessed | tf_op | source)
XLA Modules:
  0.0 165.8 jit_solution(10068222216132380455)
XLA Ops:
  0.0 164.2 %layer.1 = bf16[384,256]{1,0:T(8,128)(2,1)} custom-call(bf16[384,256]{1,0:T(8,128)(2,1)} %tok.1, f32[1,2048]{1,0:T(1,128)} %bitcast.8, bf16[64,128]{1,0:T(8,128)(2,1)} %w_sig.1, bf16[64,128]{1,0:T(8,128)(2,1)} %w_out.1, bf16[64,128]{1,0:T(8,128)(2,1)} %w_inn.1, f32[3,128]{1,0:T(4,128)} %mix_taps.1, bf16[64,128]{1,0:T(8,128)(2,1)} %bitcast.6, ...), custom_call_target="tpu_custom_call" | custom-call | tf_op jit(solution)/shard_map/layer/pallas_call | solution.py:395
  164.2 1.6 copy.15

commit v3 on v2

--- a/solution.py
+++ b/solution.py
@@ -15,7 +15,7 @@
 ONE = {"m": 2, "g": 4, "d": 1}
 BOTH = {"m": 0, "g": 2, "d": 3}
 UP_M, UP_F = 16, 16
-MIXER_AT = 8
+MIXER_AT = 11
 
 
 def conv_positions(values, taps, length):
@@ -95,14 +95,14 @@
         if col != (1 if name == "m" else 0):
             remote(part, part, push_send.at[k], push_recv.at[k], mate).start()
 
-    def mixer_step(way, first, upto):
-        for dist in (first, first + 1):
-            @pl.when(dist <= upto)
-            def _(dist=dist):
-                for col in (0, 1):
+    def mixer_step(i):
+        dist = i + 1
+        for col in (0, 1):
+            for way in (0, 1):
+                @pl.when(dist <= most["m"][way])
+                def _(way=way):
                     landed("m", col, way, dist)
-                    pl.when(dist + 2 <= upto)(lambda: send("m", col, way, dist, 2))
-                for col in (0, 1):
+                    pl.when(dist + 1 <= most["m"][way])(lambda: send("m", col, way, dist, 1))
                     spread("m", col, way, dist)
 
     def bulk_step(i):
@@ -121,18 +121,16 @@
             for way in (0, 1):
                 if kind == "m":
                     send("m", col, way, 0, 1)
-                    send("m", col, way, 0, 2)
                 else:
                     for name in ("g", "d"):
                         send(name, col, way, 0, 1)
 
-    mixer_end = (max(most["m"]) + 1) // 2
+    mixer_end = max(most["m"])
     bulk_end = max(most["g"])
 
     def mixer_steps(lo, hi):
         def body(i, _):
-            for way in (0, 1):
-                mixer_step(way, 2 * i + 1, most["m"][way])
+            mixer_step(i)
             return 0
 
         lax.fori_loop(lo, jnp.where(is_m, hi, lo), body, 0)

time: 166 us -> 155 us (0.934)
  Pallas kernels: 164 us -> 154 us
    pallas_call x1, Pallas kernels: 164 us -> 154 us  [on_device(): pl.pallas_call(functools.partial(kernel, sizes), out_shape=jax.ShapeDtype...]
where the time goes in v3:
time: 155 us
  Pallas kernels  154 us (99%)
  local copies, waits for them, and re-layouts  1.62 us (1%)
    pallas_call x1, Pallas kernels, on_device(): pl.pallas_call(functools.partial(kernel, sizes), out_shape=jax.ShapeDtype...  154 us

profile of v3, /device:TPU:33, one launch (start us, length us, event | category | flops | bytes accessed | tf_op | source)
XLA Modules:
  0.0 155.1 jit_solution(1240024564870738794)
XLA Ops:
  0.0 153.5 %layer.1 = bf16[384,256]{1,0:T(8,128)(2,1)} custom-call(bf16[384,256]{1,0:T(8,128)(2,1)} %tok.1, f32[1,2048]{1,0:T(1,128)} %bitcast.8, bf16[64,128]{1,0:T(8,128)(2,1)} %w_sig.1, bf16[64,128]{1,0:T(8,128)(2,1)} %w_out.1, bf16[64,128]{1,0:T(8,128)(2,1)} %w_inn.1, f32[3,128]{1,0:T(4,128)} %mix_taps.1, bf16[64,128]{1,0:T(8,128)(2,1)} %bitcast.6, ...), custom_call_target="tpu_custom_call" | custom-call | tf_op jit(solution)/shard_map/layer/pallas_call | solution.py:393
  153.5 1.6 %copy.15 = bf16[384,256]{1,0:T(8,128)(2,1)} copy(bf16[384,256]{1,0:T(8,128)(2,1)} %layer.1) | data formatting | bytes 393216

commit v4 on v3

--- a/solution.py
+++ b/solution.py
@@ -298,8 +298,6 @@
     three = dot(normed[...], wide).astype(BF16).astype(F32)
     signal, outer, inner = (three[:, k * LANES : (k + 1) * LANES] for k in range(3))
     mixed = (outer * conv_positions(inner * signal, mix_taps[...], length)).astype(BF16)
-
-    done = bulk_steps(done, done + 1)
 
     def mix_term(b):
         return dot_nt(mixed, gm[c, 3, pl.ds(pl.multiple_of(b * db, db), db), :])

time: 155 us -> 156 us (level)
  no operation moved by 1% of the time
where the time goes in v4:
time: 156 us
  Pallas kernels  154 us (99%)
  local copies, waits for them, and re-layouts  1.62 us (1%)
    pallas_call x1, Pallas kernels, on_device(): pl.pallas_call(functools.partial(kernel, sizes), out_shape=jax.ShapeDtype...  154 us

profile of v4, /device:TPU:33, one launch (start us, length us, event | category | flops | bytes accessed | tf_op | source)
XLA Modules:
  0.0 155.8 jit_solution(10483898881330996647)
XLA Ops:
  0.0 154.2 %layer.1 = bf16[384,256]{1,0:T(8,128)(2,1)} custom-call(bf16[384,256]{1,0:T(8,128)(2,1)} %tok.1, f32[1,2048]{1,0:T(1,128)} %bitcast.8, bf16[64,128]{1,0:T(8,128)(2,1)} %w_sig.1, bf16[64,128]{1,0:T(8,128)(2,1)} %w_out.1, bf16[64,128]{1,0:T(8,128)(2,1)} %w_inn.1, f32[3,128]{1,0:T(4,128)} %mix_taps.1, bf16[64,128]{1,0:T(8,128)(2,1)} %bitcast.6, ...), custom_call_target="tpu_custom_call" | custom-call | tf_op jit(solution)/shard_map/layer/pallas_call | solution.py:391
  154.2 1.6 %copy.15 = bf16[384,256]{1,0:T(8,128)(2,1)} copy(bf16[384,256]{1,0:T(8,128)(2,1)} %layer.1) | data formatting | bytes 393216
